TPU v7x, 32 devices: a whole 2x2x4 slice. The times are simulated.
32 devices in a mesh: fs: 16 (over z, y, x), tp: 2 (over core).
Axes of the slice: x: 2, y: 2, z: 4, core: 2. Of those that a mesh axis runs over, the one named last changes fastest.
Arguments:
- tokens: bfloat16 [12288, 2048], P('fs'), may hold values from -6 to 6
- norm_gain: float32 [2048], replicated, may hold values from 0.1 to 1.9
- up_weight: float32 [2048, 8192], P('fs', 'tp'), may hold values from -0.125 to 0.125
- up_scale: float32 [8192], P('tp'), may hold values from 0.5 to 2
- down_weight: float32 [8192, 2048], P('tp', 'fs'), may hold values from -0.0625 to 0.0625
- down_scale: float32 [2048], P('fs'), may hold values from 0.5 to 2
Outputs:
- output: bfloat16 [12288, 2048], P('fs', 'tp')
All inputs are finite; a program needn't handle non-finite values.
Results may differ from a plain program's by a relative error of at most 0.015.
Values may be sent and summed in bfloat16 or wider, within the bound.
A program may use at most 128 MiB of HBM per device.

v0:
```python
import jax
import jax.numpy as jnp
from jax import lax
from jax.sharding import PartitionSpec as P

epsilon = 1e-06


def local(tokens, norm_gain, up_weight, up_scale, down_weight, down_scale):
    floats = tokens.astype(jnp.float32)
    inverse = lax.rsqrt(jnp.mean(floats * floats, axis=-1, keepdims=True) + epsilon)
    normed = (floats * inverse * norm_gain).astype(jnp.bfloat16)
    up_half = up_weight.astype(jnp.bfloat16)
    down_half = down_weight.astype(jnp.bfloat16)
    up_pre = jnp.dot(
        normed,
        lax.all_gather(up_half, "fs", axis=0, tiled=True),
        preferred_element_type=jnp.float32,
    )
    down_whole, scale_whole = (
        lax.all_gather(down_half, "fs", axis=1, tiled=True),
        lax.all_gather(down_scale.astype(jnp.bfloat16), "fs", axis=0, tiled=True).astype(
            down_scale.dtype
        ),
    )
    hidden = jnp.square(jax.nn.relu(up_pre * up_scale)).astype(jnp.bfloat16)
    partial_value = jnp.dot(hidden, down_whole, preferred_element_type=jnp.float32).astype(
        jnp.bfloat16
    )
    summed = lax.psum_scatter(
        partial_value.astype(jnp.float32).astype(jnp.bfloat16),
        "tp",
        scatter_dimension=1,
        tiled=True,
    ).astype(jnp.float32)
    own_width = summed.shape[1]
    own_scale = lax.dynamic_slice_in_dim(
        scale_whole, lax.axis_index("tp") * own_width, own_width, 0
    )
    return (summed * own_scale).astype(jnp.bfloat16)


def solution(mesh):
    in_specs = (P("fs", None), P(), P("fs", "tp"), P("tp"), P("tp", "fs"), P("fs"))
    out_specs = P("fs", "tp")
    return jax.shard_map(local, mesh=mesh, in_specs=in_specs, out_specs=out_specs, check_vma=False)
```

profile of v0, /device:TPU:0, one launch (start us, length us, event | category | flops | bytes accessed | tf_op | source)
XLA Modules:
  0.0 539.5 jit_solution(17070823121638339327)
XLA Ops:
  6.5 0.0 copy-start
  6.5 0.0 copy-start.1
  6.5 0.0 copy-start.2
  6.5 0.0 all-gather.6.cloned.1.call-start
  6.5 2.8 convert_element_type.36
  9.4 0.0 all-gather.6.cloned.1.call-update
  9.4 0.0 all-gather.4.cloned.1.call-start
  9.4 2.7 convert_element_type.34
  12.1 0.0 all-gather.4.cloned.1.call-update
  12.2 0.0 reduce-scatter.2.cloned.1.call-start
  12.2 0.0 copy-done
  12.2 0.7 fusion
  12.9 0.0 copy-start.3
  12.9 249.0 %all-gather.6.cloned.1.call-done = bf16[4096,2048]{1,0:T(8,128)(2,1)} async-done(((bf16[4096,128]{1,0:T(8,128)(2,1)}), bf16[4096,2048]{1,0:T(8,128)(2,1)}) %all-gather.6.cloned.1.call-update) | async-done | bytes 16777232 | tf_op jit(solution)/shard_map/all_gather | solution.py:21
  261.9 192.0 %all-gather.4.cloned.1.call-done = bf16[2048,4096]{1,0:T(8,128)(2,1)} async-done(((bf16[128,4096]{1,0:T(8,128)(2,1)}), bf16[2048,4096]{1,0:T(8,128)(2,1)}) %all-gather.4.cloned.1.call-update) | async-done | bytes 16777232 | tf_op jit(solution)/shard_map/all_gather | solution.py:17
  453.9 0.0 copy-done.1
  453.9 0.0 copy-done.2
  453.9 38.2 %convolution_convert_fusion = bf16[768,2048]{1,0:T(8,128)(2,1)} fusion(bf16[4096,2048]{1,0:T(8,128)(2,1)} %all-gather.6.cloned.1.call-done, bf16[2048,4096]{1,0:T(8,128)(2,1)} %all-gather.4.cloned.1.call-done, f32[4096]{0:T(1024)S(1)} %copy-done.1, bf16[768,2048]{1,0:T(8,128)(2,1)S(1)} %copy-done, f32[2048]{0:T(1024)S(1)} %copy-done.2, ...), kind=kOutput, calls=%fused_computation.6 | convolution fusion | flops 25790251008 | bytes 39873536 | tf_op jit(solution)/shard_map/dot_general | solution.py:27
  492.1 0.0 reduce-scatter.2.cloned.1.call-update
  492.2 0.0 copy-done.3
  492.2 37.8 %all-gather = bf16[16,1,128]{2,1,0:T(2,128)(2,1)S(1)} all-gather(bf16[1,1,128]{2,1,0:T(2,128)(2,1)S(1)} %convert_bitcast_fusion), channel_id=1, replica_groups=mesh['fs'=16,'tp'=2] {'fs'}, dimensions={0}, use_global_device_ids=true | all-gather | bytes 4352 | tf_op jit(solution)/shard_map/all_gather | solution.py:22
  530.0 0.0 reduce-scatter.2.cloned.1.call-done
  530.0 3.0 multiply_convert_fusion.1
  (4 shorter events, 0.0 us)
Async XLA Ops:
  6.5 5.7 %copy-start = (bf16[768,2048]{1,0:T(8,128)(2,1)S(1)}, bf16[768,2048]{1,0:T(8,128)(2,1)}, u32[]{:S(2)}) copy-start(bf16[768,2048]{1,0:T(8,128)(2,1)} %param.6) | copy-start | bytes 9437188
  6.5 447.4 %copy-start.1 = (f32[4096]{0:T(1024)S(1)}, f32[4096]{0:T(1024)}, u32[]{:S(2)}) copy-start(f32[4096]{0:T(1024)} %param.9) | copy-start | bytes 49156
  6.5 447.4 %copy-start.2 = (f32[2048]{0:T(1024)S(1)}, f32[2048]{0:T(1024)}, u32[]{:S(2)}) copy-start(f32[2048]{0:T(1024)} %param.7) | copy-start | bytes 24580
  6.5 255.4 %all-gather.6.cloned.1.call-start = ((), (), s32[]{:S(2)}) async-start(), calls=%async_computation.2 | async-start | bytes 17825792 | tf_op jit(solution)/shard_map/all_gather | solution.py:21
  9.4 444.5 %all-gather.4.cloned.1.call-start = ((), (), s32[]{:S(2)}) async-start(), calls=%async_computation.1 | async-start | bytes 17825792 | tf_op jit(solution)/shard_map/all_gather | solution.py:17
  12.2 517.9 %reduce-scatter.2.cloned.1.call-start = ((), (), s32[]{:S(2)}) async-start(), calls=%async_computation.3 | async-start | bytes 4718592 | tf_op jit(solution)/shard_map/reduce_scatter | solution.py:30
  12.9 479.3 %copy-start.3 = (f32[128]{0:T(128)S(1)}, f32[128]{0:T(128)}, u32[]{:S(2)}) copy-start(f32[128]{0:T(128)} %param.11) | copy-start | bytes 1540
Sparse Core Ops, SparseCore 0:
  10.0 251.8 all-gather.5
  264.7 189.1 all-gather.3
  492.3 9.1 reduce-scatter.1
where the time goes:
time: 540 us
  waiting for transfers between devices  441 us (82%)
  matrix products  38.2 us (7%)
  blocking collectives  37.8 us (7%)
  between operations  13.2 us (2%)
  other arithmetic  9.18 us (2%)
    all_gather x1, waiting for transfers between devices, local(): lax.all_gather(down_half, 'fs', axis=1, tiled=True)  249 us
    all_gather x1, waiting for transfers between devices, local(): lax.all_gather(up_half, 'fs', axis=0, tiled=True)  192 us
    dot_general x1, matrix products, local(): jnp.dot(hidden, down_whole, preferred_element_type=jnp.float32)  38.2 us
    all_gather x1, blocking collectives, local(): lax.all_gather(down_scale.astype(jnp.bfloat16), 'fs', axis=0, tiled=True)  37.8 us
  transfers between devices with their start and end apart: 3, of which 2 were waited for; matrix products, arithmetic and copies ran while one was open for 1% of the time, Pallas kernels for 0%

commit v1 on v0

--- a/solution.py
+++ b/solution.py
@@ -4,6 +4,13 @@
 from jax.sharding import PartitionSpec as P
 
 epsilon = 1e-06
+
+
+def exchange_gather(x, name, dim):
+    size = lax.axis_size(name)
+    parts = jnp.stack([x for _ in range(size)])
+    parts = lax.all_to_all(parts, name, split_axis=0, concat_axis=0)
+    return jnp.concatenate(parts, axis=dim)
 
 
 def local(tokens, norm_gain, up_weight, up_scale, down_weight, down_scale):
@@ -18,7 +25,7 @@
         preferred_element_type=jnp.float32,
     )
     down_whole, scale_whole = (
-        lax.all_gather(down_half, "fs", axis=1, tiled=True),
+        exchange_gather(down_half, "fs", 1),
         lax.all_gather(down_scale.astype(jnp.bfloat16), "fs", axis=0, tiled=True).astype(
             down_scale.dtype
         ),

time: 540 us -> 616 us (1.14)
  waiting for transfers between devices: 441 us -> 473 us
  blocking collectives: 37.8 us -> 67.6 us
  starting transfers between devices: 0.09 us -> 8.7 us
  local copies, waits for them, and re-layouts: 0.03 us -> 6.5 us
    all_gather x1, waiting for transfers between devices: 192 us -> 473 us  [local(): lax.all_gather(up_half, 'fs', axis=0, tiled=True)]
    all_gather x1 -> x0, waiting for transfers between devices: 249 us -> none  [local(): lax.all_gather(down_half, 'fs', axis=1, tiled=True)]
    all_gather x1, blocking collectives: 37.8 us -> 67.6 us  [local(): lax.all_gather(down_scale.astype(jnp.bfloat16), 'fs', axis=0, tiled=True)]
    dot_general x0 -> x1, matrix products: none -> 18.7 us  [local(): jnp.dot(normed, lax.all_gather(up_half, 'fs', axis=0, tiled=True), prefer...]
    dot_general x1, matrix products: 38.2 us -> 19.8 us  [local(): jnp.dot(hidden, down_whole, preferred_element_type=jnp.float32)]
    all_to_all x0 -> x1, starting transfers between devices: none -> 8.66 us  [exchange_gather(): parts = lax.all_to_all(parts, name, split_axis=0, concat_axis=0)]
  transfers between devices with their start and end apart: 3 -> 3, of which waited for: 2 -> 1; matrix products, arithmetic and copies ran while one was open for 1% -> 4% of each run, Pallas kernels for 0% -> 0%
where the time goes in v1:
time: 616 us
  waiting for transfers between devices  473 us (77%)
  blocking collectives  67.6 us (11%)
  matrix products  38.4 us (6%)
  between operations  13.5 us (2%)
  starting transfers between devices  8.7 us (1%)
  other arithmetic  8.05 us (1%)
  local copies, waits for them, and re-layouts  6.5 us (1%)
    all_gather x1, waiting for transfers between devices, local(): lax.all_gather(up_half, 'fs', axis=0, tiled=True)  473 us
    all_gather x1, blocking collectives, local(): lax.all_gather(down_scale.astype(jnp.bfloat16), 'fs', axis=0, tiled=True)  67.6 us
    dot_general x1, matrix products, local(): jnp.dot(hidden, down_whole, preferred_element_type=jnp.float32)  19.8 us
    dot_general x1, matrix products, local(): jnp.dot(normed, lax.all_gather(up_half, 'fs', axis=0, tiled=True), prefer...  18.7 us
  transfers between devices with their start and end apart: 3, of which 1 were waited for; matrix products, arithmetic and copies ran while one was open for 4% of the time, Pallas kernels for 0%

profile of v1, /device:TPU:0, one launch (start us, length us, event | category | flops | bytes accessed | tf_op | source)
XLA Modules:
  0.0 615.9 jit_solution(33428019887355260)
XLA Ops:
  6.5 0.0 all-gather.3.cloned.1.call-start
  6.5 2.7 convert_element_type.34
  9.2 0.0 all-gather.3.cloned.1.call-update
  9.3 1.7 convert_element_type.36
  11.0 0.5 copy.8
  11.5 5.9 stack.2
  17.4 0.0 copy-start
  17.4 0.0 copy-start.1
  17.4 0.0 copy-start.2
  17.4 8.7 %all-to-all-start = ((bf16[16,4096,128]{1,2,0:T(8,128)(2,1)}), bf16[16,4096,128]{1,2,0:T(8,128)(2,1)}, u32[]{:S(2)}, u32[]{:S(2)}) async-start(bf16[16,4096,128]{1,2,0:T(8,128)(2,1)} %stack.2), calls=%async_computation | async-start | bytes 33554432 | tf_op jit(solution)/shard_map/all_to_all | solution.py:12
  26.1 0.0 reduce-scatter.2.cloned.1.call-start
  26.2 0.0 copy-done
  26.2 0.7 fusion
  26.9 473.1 %all-gather.3.cloned.1.call-done = bf16[2048,4096]{1,0:T(8,128)(2,1)} async-done(((bf16[128,4096]{1,0:T(8,128)(2,1)}), bf16[2048,4096]{1,0:T(8,128)(2,1)}) %all-gather.3.cloned.1.call-update) | async-done | bytes 16777232 | tf_op jit(solution)/shard_map/all_gather | solution.py:24
  500.0 0.0 copy-done.1
  500.0 0.0 copy-done.2
  500.0 18.7 %fusion.26 = bf16[768,4096]{1,0:T(8,128)(2,1)} fusion(f32[4096]{0:T(1024)S(1)} %copy-done.1, bf16[2048,4096]{1,0:T(8,128)(2,1)} %all-gather.3.cloned.1.call-done, bf16[768,2048]{1,0:T(8,128)(2,1)S(1)} %copy-done, f32[2048]{0:T(1024)S(1)} %copy-done.2, f32[768]{0:T(1024)S(1)} %add_rsqrt_fusion), kind=kOutput, calls=%bitcast_fusion.clone.1 | convolution fusion | flops 12903776256 | bytes 26242048 | tf_op jit(solution)/shard_map/dot_general | solution.py:22
  518.6 0.0 all-to-all-done
  518.6 0.0 copy-start.3
  518.6 19.8 %convolution_convert_fusion = bf16[768,2048]{1,0:T(8,128)(2,1)} fusion(bf16[4096,2048]{0,1:T(8,128)(2,1)} %bitcast.1, bf16[768,4096]{1,0:T(8,128)(2,1)} %fusion.26), kind=kOutput, calls=%fused_computation.6 | convolution fusion | flops 12886474752 | bytes 26214400 | tf_op jit(solution)/shard_map/dot_general | solution.py:34
  538.4 0.0 reduce-scatter.2.cloned.1.call-update
  538.4 0.0 copy-done.3
  538.4 67.6 %all-gather = bf16[16,1,128]{2,1,0:T(2,128)(2,1)S(1)} all-gather(bf16[1,1,128]{2,1,0:T(2,128)(2,1)S(1)} %convert_bitcast_fusion), channel_id=1, replica_groups=mesh['fs'=16,'tp'=2] {'fs'}, dimensions={0}, use_global_device_ids=true | all-gather | bytes 4352 | tf_op jit(solution)/shard_map/all_gather | solution.py:29
  606.1 0.0 reduce-scatter.2.cloned.1.call-done
  606.1 3.0 multiply_convert_fusion.1
  (4 shorter events, 0.0 us)
Async XLA Ops:
  6.5 493.4 %all-gather.3.cloned.1.call-start = ((), (), s32[]{:S(2)}) async-start(), calls=%async_computation.2 | async-start | bytes 17825792 | tf_op jit(solution)/shard_map/all_gather | solution.py:24
  17.4 8.7 %copy-start = (bf16[768,2048]{1,0:T(8,128)(2,1)S(1)}, bf16[768,2048]{1,0:T(8,128)(2,1)}, u32[]{:S(2)}) copy-start(bf16[768,2048]{1,0:T(8,128)(2,1)} %param.6) | copy-start | bytes 9437188
  17.4 482.5 %copy-start.1 = (f32[4096]{0:T(1024)S(1)}, f32[4096]{0:T(1024)}, u32[]{:S(2)}) copy-start(f32[4096]{0:T(1024)} %param.9) | copy-start | bytes 49156
  17.4 482.5 %copy-start.2 = (f32[2048]{0:T(1024)S(1)}, f32[2048]{0:T(1024)}, u32[]{:S(2)}) copy-start(f32[2048]{0:T(1024)} %param.7) | copy-start | bytes 24580
  17.4 501.2 %all-to-all-start = ((bf16[16,4096,128]{1,2,0:T(8,128)(2,1)}), bf16[16,4096,128]{1,2,0:T(8,128)(2,1)}, u32[]{:S(2)}, u32[]{:S(2)}) async-start(bf16[16,4096,128]{1,2,0:T(8,128)(2,1)} %stack.2), calls=%async_computation | async-start | bytes 33554432 | tf_op jit(solution)/shard_map/all_to_all | solution.py:12
  26.1 580.0 %reduce-scatter.2.cloned.1.call-start = ((), (), s32[]{:S(2)}) async-start(), calls=%async_computation.3 | async-start | bytes 4718592 | tf_op jit(solution)/shard_map/reduce_scatter | solution.py:37
  518.6 19.8 %copy-start.3 = (f32[128]{0:T(128)S(1)}, f32[128]{0:T(128)}, u32[]{:S(2)}) copy-start(f32[128]{0:T(128)} %param.11) | copy-start | bytes 1540
Sparse Core Ops, SparseCore 0:
  10.1 489.8 all-gather.2
  538.5 42.9 reduce-scatter.1
